TPU v7x, 256 devices: a whole 4x4x8 slice. The times are simulated.
256 devices in a mesh: ep: 64 (over z, x, core), tp: 4 (over y).
Axes of the slice: x: 4, y: 4, z: 8, core: 2. Of those that a mesh axis runs over, the one named last changes fastest.
Arguments:
- mixer_input: bfloat16 [40960, 2048], P('ep'), may hold values from -6 to 6
- mixer_gain: float32 [2048], replicated, may hold values from 0.1 to 1.9
- value_weight: bfloat16 [2048, 1024], P(None, 'tp'), may hold values from -0.125 to 0.125
- inner_gate: bfloat16 [2048, 1024], P(None, 'tp'), may hold values from -0.125 to 0.125
- outer_gate: bfloat16 [2048, 1024], P(None, 'tp'), may hold values from -0.125 to 0.125
- kernel_taps: float32 [3, 1024], P(None, 'tp'), may hold values from -3 to 3
- mixer_proj: bfloat16 [1024, 2048], P('tp'), may hold values from -0.1875 to 0.1875
- expert_input: bfloat16 [40960, 2048], P(('ep', 'tp')), may hold values from -6 to 6
- expert_gain: float32 [2048], replicated, may hold values from 0.1 to 1.9
- routes: int32 [40960, 2], P(('ep', 'tp')), may hold values from 0 to 63, as said below
- group_logits: float32 [40960, 8], P(('ep', 'tp')), may hold values from -6 to 6
- pair_logits: float32 [40960, 2], P(('ep', 'tp')), may hold values from -6 to 6
- gate_weight: bfloat16 [64, 2048, 1024], P('ep', None, 'tp'), may hold values from -0.125 to 0.125
- up_weight: bfloat16 [64, 2048, 1024], P('ep', None, 'tp'), may hold values from -0.125 to 0.125
- down_weight: bfloat16 [64, 1024, 2048], P('ep', 'tp'), may hold values from -0.75 to 0.75
Outputs:
- mixer_output: bfloat16 [40960, 2048], P(('ep', 'tp'))
- expert_output: bfloat16 [40960, 2048], P(('ep', 'tp'))
Inputs may be any that keep to these rules, and one draw needn't show every extreme that they name: `routes`: both entries of a row are different experts of one group (equal after integer division by 8). In the rows of one device every group is chosen by the same number of rows, no expert is named more than 10 times, and in every draw one expert is named exactly 10 times in the rows of every device.
All inputs are finite; a program needn't handle non-finite values.
Results may differ from a plain program's by a relative error of at most 0.01.
Values may be sent and summed in bfloat16 or wider, within the bound.
A program may use at most 128 MiB of HBM per device.

v0:
```python
import jax
import jax.numpy as jnp
from jax import lax
from jax.sharding import PartitionSpec as P

EPG = 8
EPSILON = 1e-06


def padded_2(cells, axis):
    count = lax.axis_size(axis)
    ends = count - 1
    head = cells[:1]
    tail = cells[-1:]
    return jnp.concatenate(
        [
            lax.ppermute(tail, axis, [(i, i + 1) for i in range(ends)]),
            cells,
            lax.ppermute(head, axis, [(i + 1, i) for i in range(ends)]),
        ],
        axis=0,
    )


def normed(values, gain):
    wide = values.astype(jnp.float32)
    scale = lax.rsqrt(jnp.mean(wide * wide, axis=-1, keepdims=True) + EPSILON)
    return (wide * scale * gain).astype(jnp.bfloat16)


def route_weights(routes, group_logits, pair_logits):
    chosen = routes[:, 0] // EPG
    groups = jnp.arange(group_logits.shape[1], dtype=jnp.int32)
    picked = jnp.sum(jnp.where(groups[None, :] == chosen[:, None], group_logits, 0.0), axis=1)
    group_weight = 1.0 / jnp.sum(jnp.exp(group_logits - picked[:, None]), axis=1)
    return group_weight[:, None] * jax.nn.sigmoid(pair_logits - pair_logits[:, ::-1])


def f32dot(a, b):
    return jnp.dot(a, b, preferred_element_type=jnp.float32)


def on_device(
    mixer_input,
    mixer_gain,
    value_weight,
    inner_gate,
    outer_gate,
    kernel_taps,
    mixer_proj,
    expert_input,
    expert_gain,
    routes,
    group_logits,
    pair_logits,
    gate_weight,
    up_weight,
    down_weight,
):
    split = lax.axis_size("tp")
    experts = lax.axis_size("ep")
    n_groups = experts // EPG
    local = expert_input.shape[0]
    width = expert_input.shape[1]
    per = local // n_groups
    expert_norm = normed(expert_input, expert_gain)
    weights = route_weights(routes, group_logits, pair_logits)
    member = routes % EPG
    lanes = jnp.arange(EPG, dtype=jnp.int32)
    wide_w = jnp.where(member[:, 0:1] == lanes, weights[:, 0:1], 0.0) + jnp.where(
        member[:, 1:2] == lanes, weights[:, 1:2], 0.0
    )
    high = wide_w.astype(jnp.bfloat16)
    low = (wide_w - high.astype(jnp.float32)).astype(jnp.bfloat16)
    extra = jnp.concatenate([high, low, jnp.zeros((local, 128 - 2 * EPG), jnp.bfloat16)], axis=1)
    group = routes[:, 0] // EPG
    place = jnp.arange(local, dtype=jnp.int32)
    earlier = (group[:, None] == group[None, :]) & (place[None, :] < place[:, None])
    slot = group * per + jnp.sum(earlier.astype(jnp.int32), axis=1)
    onehot = (slot[:, None] == place[None, :]).astype(jnp.bfloat16)
    rows = jnp.concatenate([expert_norm, extra], axis=1)
    ordered = lax.dot_general(
        onehot, rows, (((0,), (0,)), ((), ())), preferred_element_type=jnp.float32
    ).astype(jnp.bfloat16)
    z_groups = [[z * EPG + i for z in range(n_groups)] for i in range(EPG)]
    plane_groups = [[z * EPG + i for i in range(EPG)] for z in range(n_groups)]
    arrived = lax.all_to_all(
        ordered, "ep", split_axis=0, concat_axis=0, axis_index_groups=z_groups, tiled=True
    )
    everyone = lax.all_gather(arrived, "ep", axis=0, axis_index_groups=plane_groups, tiled=True)
    all_gate = lax.all_gather(gate_weight[0], "tp", axis=0)
    all_up = lax.all_gather(up_weight[0], "tp", axis=0)
    all_down = lax.all_gather(down_weight[0], "tp", axis=0, tiled=True)
    normal_rows = normed(mixer_input, mixer_gain)
    values = f32dot(normal_rows, value_weight)
    inner = f32dot(normal_rows, inner_gate)
    outer = f32dot(normal_rows, outer_gate)
    mixed_in = (inner * values).astype(jnp.bfloat16)
    padded = padded_2(mixed_in, "ep").astype(jnp.float32)
    conv_sum = (
        kernel_taps[0] * padded[:-2] + kernel_taps[1] * padded[1:-1] + kernel_taps[2] * padded[2:]
    )
    mixer_rows = (outer * conv_sum).astype(jnp.bfloat16)
    partial = f32dot(mixer_rows, mixer_proj).astype(jnp.bfloat16)
    blocks = lax.all_to_all(partial.reshape(split, -1, width), "tp", 0, 0, tiled=True)
    mixer_output = jnp.sum(blocks.astype(jnp.float32), axis=0).astype(jnp.bfloat16)
    tokens = everyone[:, :width]
    mine = lax.axis_index("ep") % EPG
    both = everyone[:, width:].astype(jnp.float32)
    spot = jnp.arange(128, dtype=jnp.int32)
    weight = jnp.sum(
        jnp.where((spot == mine) | (spot == mine + EPG), both, 0.0), axis=1, keepdims=True
    )
    parts = []
    for j in range(split):
        first = f32dot(tokens, all_gate[j])
        second = f32dot(tokens, all_up[j])
        parts.append((jax.nn.silu(first) * second).astype(jnp.bfloat16))
    hidden = jnp.concatenate(parts, axis=1)
    answers = (f32dot(hidden, all_down) * weight).astype(jnp.bfloat16)
    home = lax.psum_scatter(
        answers, "ep", scatter_dimension=0, axis_index_groups=plane_groups, tiled=True
    )
    back = lax.all_to_all(
        home, "ep", split_axis=0, concat_axis=0, axis_index_groups=z_groups, tiled=True
    )
    expert_output = f32dot(onehot, back).astype(jnp.bfloat16)
    return (mixer_output, expert_output)


def solution(mesh):
    in_specs = (
        P("ep", None),
        P(),
        P(None, "tp"),
        P(None, "tp"),
        P(None, "tp"),
        P(None, "tp"),
        P("tp", None),
        P(("ep", "tp"), None),
        P(),
        P(("ep", "tp"), None),
        P(("ep", "tp"), None),
        P(("ep", "tp"), None),
        P("ep", None, "tp"),
        P("ep", None, "tp"),
        P("ep", "tp", None),
    )
    out_specs = (P(("ep", "tp"), None), P(("ep", "tp"), None))
    return jax.shard_map(
        on_device, mesh=mesh, in_specs=in_specs, out_specs=out_specs, check_vma=False
    )
```

profile of v0, /device:TPU:3, one launch (start us, length us, event | category | flops | bytes accessed | tf_op | source)
XLA Modules:
  0.0 350.5 jit_solution(15072283598216035923)
XLA Ops:
  7.2 0.0 copy-start
  7.2 0.0 all-gather.6.cloned.1.call-start
  7.2 0.8 fusion.52
  8.0 0.7 and_select_fusion
  8.7 0.7 select_reduce_fusion.1
  9.4 0.7 exponential_reduce_fusion
  10.1 0.7 rev.3
  10.9 0.7 divide_multiply_fusion
  11.6 0.1 copy.23
  11.7 0.1 copy.24
  11.8 1.3 fusion.15
  13.2 0.2 convert_reduce_fusion
  13.4 1.3 fusion.17
  14.7 0.3 concatenate.10
  15.0 0.5 convolution_convert_fusion
  15.5 0.1 all_to_all.20
  15.6 30.7 %all_to_all.29 = bf16[8,20,2176]{2,1,0:T(8,128)(2,1)S(1)} all-to-all(bf16[8,20,2176]{2,1,0:T(8,128)(2,1)S(1)} %all_to_all.20), channel_id=1, replica_groups={{0,32,64,96,128,160,192,224},{4,36,68,100,132,164,196,228},{8,40,72,104..., dimensions={0} | all-to-all | bytes 1392640 | tf_op jit(solution)/shard_map/all_to_all | solution.py:87
  46.3 1.0 all_to_all.22
  47.3 0.0 all-gather.6.cloned.1.call-update
  47.3 0.0 all-gather.8.cloned.1.call-start
  47.4 0.7 all-gather.8.cloned.1.call-update
  48.1 0.0 all-gather.10.cloned.1.call-start
  48.1 0.7 all-gather.10.cloned.1.call-update
  48.8 0.0 all-gather.12.cloned.1.call-start
  48.9 0.5 all-gather.12.cloned.1.call-update
  49.4 0.0 reduce-scatter.2.cloned.1.call-start
  49.5 35.9 %all-gather.6.cloned.1.call-done = bf16[1280,2176]{1,0:T(8,128)(2,1)} async-done(((bf16[160,2176]{1,0:T(8,128)(2,1)}), bf16[1280,2176]{1,0:T(8,128)(2,1)}) %all-gather.6.cloned.1.call-update) | async-done | bytes 5570576 | tf_op jit(solution)/shard_map/all_gather | solution.py:90
  85.4 1.1 select_reduce_fusion
  86.5 51.9 %all-gather.8.cloned.1.call-done = bf16[4,2048,256]{2,1,0:T(8,128)(2,1)} async-done(((bf16[1,2048,256]{2,1,0:T(8,128)(2,1)}), bf16[4,2048,256]{2,1,0:T(8,128)(2,1)}) %all-gather.8.cloned.1.call-update) | async-done | bytes 4194320 | tf_op jit(solution)/shard_map/all_gather | solution.py:91
  138.4 5.5 %fusion.23 = f32[1280,256]{0,1:T(8,128)} fusion(bf16[4,2048,256]{2,1,0:T(8,128)(2,1)} %all-gather.8.cloned.1.call-done, bf16[1280,2176]{1,0:T(8,128)(2,1)} %all-gather.6.cloned.1.call-done), kind=kOutput, calls=%fused_computation.45 | convolution fusion | flops 1342177280 | bytes 7602176 | tf_op jit(solution)/shard_map/dot_general | solution.py:40
  144.0 0.6 copy-done.5
  144.6 2.7 fusion.22
  147.3 2.7 fusion.21
  150.0 1.6 fusion.20
  151.6 39.8 %all-gather.10.cloned.1.call-done = bf16[4,2048,256]{2,1,0:T(8,128)(2,1)} async-done(((bf16[1,2048,256]{2,1,0:T(8,128)(2,1)}), bf16[4,2048,256]{2,1,0:T(8,128)(2,1)}) %all-gather.10.cloned.1.call-update) | async-done | bytes 4194320 | tf_op jit(solution)/shard_map/all_gather | solution.py:92
  191.4 5.0 %fusion.11 = bf16[1280,256]{0,1:T(8,128)(2,1)S(1)} fusion(f32[1280,256]{0,1:T(8,128)} %fusion.23, bf16[4,2048,256]{2,1,0:T(8,128)(2,1)} %all-gather.10.cloned.1.call-done, bf16[1280,2176]{1,0:T(8,128)(2,1)} %all-gather.6.cloned.1.call-done), kind=kOutput, calls=%fused_computation.20 | convolution fusion | flops 1344143360 | bytes 8257536 | tf_op jit(solution)/shard_map/dot_general | solution.py:40
  196.4 0.0 slice-start.1
  196.4 5.2 %fusion.12 = bf16[1280,256]{0,1:T(8,128)(2,1)} fusion(f32[1280,256]{0,1:T(8,128)S(1)} %copy-done.9, bf16[4,2048,256]{2,1,0:T(8,128)(2,1)S(1)} %copy-done.4, bf16[1280,2176]{1,0:T(8,128)(2,1)} %all-gather.6.cloned.1.call-done), kind=kOutput, calls=%fused_computation.21 | convolution fusion | flops 1344143360 | bytes 8257536 | tf_op jit(solution)/shard_map/dot_general | solution.py:40
  201.7 2.6 fusion.13
  204.3 2.8 fusion.14
  207.1 37.1 %all-gather.12.cloned.1.call-done = bf16[1,1024,2048]{2,1,0:T(8,128)(2,1)} async-done(((bf16[1,256,2048]{2,1,0:T(8,128)(2,1)}), bf16[1,1024,2048]{2,1,0:T(8,128)(2,1)}) %all-gather.12.cloned.1.call-update) | async-done | bytes 4194320 | tf_op jit(solution)/shard_map/all_gather | solution.py:93
  244.2 9.9 %multiply_convert_fusion = bf16[1280,2048]{1,0:T(8,128)(2,1)} fusion(f32[1280]{0:T(1024)S(1)} %select_reduce_fusion, bf16[1,1024,2048]{2,1,0:T(8,128)(2,1)} %all-gather.12.cloned.1.call-done, bf16[1280,256]{0,1:T(8,128)(2,1)} %fusion.14, bf16[1280,256]{0,1:T(8,128)(2,1)} %fusion.13, bf16[1280,256]{0,1:T(8,128)(2,1)} %fusion.12, bf16[1280,256]{0,1:T(8,128)(2,1)S(1)} %fusion.11), kind=kOutput, calls=%fused_computation | convolution fusion | flops 5384437760 | bytes 12063744 | tf_op jit(solution)/shard_map/dot_general | solution.py:40
  254.1 0.0 reduce-scatter.2.cloned.1.call-update
  254.2 2.3 fusion
  256.5 0.0 copy-start.1
  256.5 0.0 copy-start.6
  256.5 3.1 fusion.46
  259.6 0.0 copy-done.6
  259.6 0.9 fusion.19
  260.6 3.8 %collective-permute-start = (bf16[1,256]{1,0:T(2,128)(2,1)S(1)}, bf16[1,256]{1,0:T(2,128)(2,1)S(1)}, u32[]{:S(2)}, u32[]{:S(2)}) collective-permute-start(bf16[1,256]{1,0:T(2,128)(2,1)S(1)} %get-tuple-element.2), channel_id=1, source_target_pairs={{0,4},{4,8},{8,12},{12,16},{16,20},{20,24},{24,28},{28,32},{32,36}... | collective-permute-start | bytes 1544 | tf_op jit(solution)/shard_map/ppermute | solution.py:17
  264.4 1.9 collective-permute-start.1
  266.3 0.0 collective-permute-done
  266.3 3.3 collective-permute-done.1
  269.7 0.1 maximum_convert_fusion
  269.8 6.5 %convolution_convert_fusion.1 = bf16[640,2048]{1,0:T(8,128)(2,1)} fusion(bf16[256,2048]{1,0:T(8,128)(2,1)S(1)} %copy-done, bf16[2048,256]{1,0:T(8,128)(2,1)} %param.19, f32[642,256]{1,0:T(8,128)S(1)} %maximum_convert_fusion, f32[256]{0:T(256)S(1)} %bitcast.59, f32[256]{0:T(256)S(1)} %bitcast.60, f32[256]{0:T(256)S(1)} %bitcast.58, ...), kind=kOutput, calls=%fused_computation.8 | convolution fusion | flops 1349877760 | bytes 9321472 | tf_op jit(solution)/shard_map/dot_general | solution.py:40
  276.3 4.6 %all-to-all-start = ((bf16[4,160,2048]{2,1,0:T(8,128)(2,1)}), bf16[4,160,2048]{2,1,0:T(8,128)(2,1)}, u32[]{:S(2)}, u32[]{:S(2)}) async-start(bf16[4,160,2048]{2,1,0:T(8,128)(2,1)} %bitcast.45), calls=%async_computation | async-start | bytes 5242880 | tf_op jit(solution)/shard_map/all_to_all | solution.py:105
  280.9 13.4 %reduce-scatter.2.cloned.1.call-done = bf16[160,2048]{1,0:T(8,128)(2,1)} async-done(((bf16[1280,2048]{1,0:T(8,128)(2,1)}), bf16[160,2048]{1,0:T(8,128)(2,1)}) %reduce-scatter.2.cloned.1.call-update) | async-done | bytes 655376 | tf_op jit(solution)/shard_map/reduce_scatter | solution.py:121
  294.3 2.0 all_to_all.23
  296.4 15.8 %all-to-all-done = bf16[4,160,2048]{2,1,0:T(8,128)(2,1)} async-done(((bf16[4,160,2048]{2,1,0:T(8,128)(2,1)}), bf16[4,160,2048]{2,1,0:T(8,128)(2,1)}, u32[]{:S(2)}, u32[]{:S(2)}) %all-to-all-start) | async-done | bytes 2621472 | tf_op jit(solution)/shard_map/all_to_all | solution.py:105
  312.2 6.7 %all-to-all-start.2 = ((bf16[8,20,2048]{2,1,0:T(8,128)(2,1)}), bf16[8,20,2048]{2,1,0:T(8,128)(2,1)S(1)}, u32[]{:S(2)}, u32[]{:S(2)}) async-start(bf16[8,20,2048]{2,1,0:T(8,128)(2,1)} %all_to_all.23), calls=%async_computation.3 | async-start | bytes 1572864 | tf_op jit(solution)/shard_map/all_to_all | solution.py:124
  318.9 3.3 reduce_sum.69
  322.1 20.4 %all-to-all-done.2 = bf16[8,20,2048]{2,1,0:T(8,128)(2,1)S(1)} async-done(((bf16[8,20,2048]{2,1,0:T(8,128)(2,1)}), bf16[8,20,2048]{2,1,0:T(8,128)(2,1)S(1)}, u32[]{:S(2)}, u32[]{:S(2)}) %all-to-all-start.2) | async-done | bytes 655392 | tf_op jit(solution)/shard_map/all_to_all | solution.py:124
  342.6 0.1 all_to_all.25
  342.7 1.2 convolution_convert_fusion.2
  (31 shorter events, 0.1 us)
Async XLA Ops:
  7.2 262.6 %copy-start = (bf16[256,2048]{1,0:T(8,128)(2,1)S(1)}, bf16[256,2048]{1,0:T(8,128)(2,1)}, u32[]{:S(2)}) copy-start(bf16[256,2048]{1,0:T(8,128)(2,1)} %param.21) | copy-start | bytes 3145732
  7.2 78.2 %all-gather.6.cloned.1.call-start = ((), (), s32[]{:S(2)}) async-start(), calls=%async_computation.4 | async-start | bytes 6266880 | tf_op jit(solution)/shard_map/all_gather | solution.py:90
  47.3 91.1 %all-gather.8.cloned.1.call-start = ((), (), s32[]{:S(2)}) async-start(), calls=%async_computation.5 | async-start | bytes 5242880 | tf_op jit(solution)/shard_map/all_gather | solution.py:91
  48.1 143.3 %all-gather.10.cloned.1.call-start = ((), (), s32[]{:S(2)}) async-start(), calls=%async_computation.6 | async-start | bytes 5242880 | tf_op jit(solution)/shard_map/all_gather | solution.py:92
  48.8 195.4 %all-gather.12.cloned.1.call-start = ((), (), s32[]{:S(2)}) async-start(), calls=%async_computation.8 | async-start | bytes 5242880 | tf_op jit(solution)/shard_map/all_gather | solution.py:93
  49.4 244.9 %reduce-scatter.2.cloned.1.call-start = ((), (), s32[]{:S(2)}) async-start(), calls=%async_computation.7 | async-start | bytes 5898240 | tf_op jit(solution)/shard_map/reduce_scatter | solution.py:121
  138.4 5.6 %copy-start.2 = (bf16[1280,2176]{1,0:T(8,128)(2,1)S(1)}, bf16[1280,2176]{1,0:T(8,128)(2,1)}, u32[]{:S(2)}) copy-start(bf16[1280,2176]{1,0:T(8,128)(2,1)} %all-gather.6.cloned.1.call-done) | copy-start | bytes 16711684
  138.4 6.1 %copy-start.5 = (bf16[4,2048,256]{2,1,0:T(8,128)(2,1)S(1)}, bf16[4,2048,256]{2,1,0:T(8,128)(2,1)}, u32[]{:S(2)}) copy-start(bf16[4,2048,256]{2,1,0:T(8,128)(2,1)} %all-gather.8.cloned.1.call-done) | copy-start | bytes 12582916
  191.4 5.0 %copy-start.4 = (bf16[4,2048,256]{2,1,0:T(8,128)(2,1)S(1)}, bf16[4,2048,256]{2,1,0:T(8,128)(2,1)}, u32[]{:S(2)}) copy-start(bf16[4,2048,256]{2,1,0:T(8,128)(2,1)} %all-gather.10.cloned.1.call-done) | copy-start | bytes 12582916
  191.4 5.0 %copy-start.9 = (f32[1280,256]{0,1:T(8,128)S(1)}, f32[1280,256]{0,1:T(8,128)}, u32[]{:S(2)}) copy-start(f32[1280,256]{0,1:T(8,128)} %fusion.22) | copy-start | bytes 3932164
  191.4 10.3 %slice-start = ((s8[5570560]{0:T(1024)(128)(4,1)}), s8[4194304]{0:T(1024)(128)(4,1)S(1)}, s32[]{:S(2)}) async-start(s8[5570560]{0:T(1024)(128)(4,1)} %bitcast.46), calls=%async_computation.9 | async-start | bytes 8388608
  196.4 5.3 %slice-start.1 = ((s8[5570560]{0:T(1024)(128)(4,1)}), s8[1376256]{0:T(1024)(128)(4,1)S(1)}, s32[]{:S(2)}) async-start(s8[5570560]{0:T(1024)(128)(4,1)} %bitcast.46), calls=%async_computation.10 | async-start | bytes 2752512
  196.4 5.3 %copy-start.8 = (f32[1280,256]{0,1:T(8,128)S(1)}, f32[1280,256]{0,1:T(8,128)}, u32[]{:S(2)}) copy-start(f32[1280,256]{0,1:T(8,128)} %fusion.21) | copy-start | bytes 3932164
  254.1 2.4 copy-start.7
  256.5 3.1 copy-start.1
  256.5 3.1 copy-start.6
  259.6 6.7 %copy-start.3 = (f32[3,256]{1,0:T(4,128)S(1)}, f32[3,256]{1,0:T(4,128)}, u32[]{:S(2)}) copy-start(f32[3,256]{1,0:T(4,128)} %param.20) | copy-start | bytes 9220
  260.6 5.8 %collective-permute-start = (bf16[1,256]{1,0:T(2,128)(2,1)S(1)}, bf16[1,256]{1,0:T(2,128)(2,1)S(1)}, u32[]{:S(2)}, u32[]{:S(2)}) collective-permute-start(bf16[1,256]{1,0:T(2,128)(2,1)S(1)} %get-tuple-element.2), channel_id=1, source_target_pairs={{0,4},{4,8},{8,12},{12,16},{16,20},{20,24},{24,28},{28,32},{32,36}... | collective-permute-start | bytes 1544 | tf_op jit(solution)/shard_map/ppermute | solution.py:17
  264.4 5.3 %collective-permute-start.1 = (bf16[1,256]{1,0:T(2,128)(2,1)S(1)}, bf16[1,256]{1,0:T(2,128)(2,1)S(1)}, u32[]{:S(2)}, u32[]{:S(2)}) collective-permute-start(bf16[1,256]{1,0:T(2,128)(2,1)S(1)} %get-tuple-element.3), channel_id=1, source_target_pairs={{4,0},{8,4},{12,8},{16,12},{20,16},{24,20},{28,24},{32,28},{36,32}... | collective-permute-start | bytes 1544 | tf_op jit(solution)/shard_map/ppermute | solution.py:19
  276.3 35.9 %all-to-all-start = ((bf16[4,160,2048]{2,1,0:T(8,128)(2,1)}), bf16[4,160,2048]{2,1,0:T(8,128)(2,1)}, u32[]{:S(2)}, u32[]{:S(2)}) async-start(bf16[4,160,2048]{2,1,0:T(8,128)(2,1)} %bitcast.45), calls=%async_computation | async-start | bytes 5242880 | tf_op jit(solution)/shard_map/all_to_all | solution.py:105
  312.2 30.4 %all-to-all-start.2 = ((bf16[8,20,2048]{2,1,0:T(8,128)(2,1)}), bf16[8,20,2048]{2,1,0:T(8,128)(2,1)S(1)}, u32[]{:S(2)}, u32[]{:S(2)}) async-start(bf16[8,20,2048]{2,1,0:T(8,128)(2,1)} %all_to_all.23), calls=%async_computation.3 | async-start | bytes 1572864 | tf_op jit(solution)/shard_map/all_to_all | solution.py:124
Sparse Core Ops, SparseCore 0:
  47.5 37.8 all-gather.5
  87.2 51.2 all-gather.7
  140.2 51.1 all-gather.9
  193.1 51.1 all-gather.11
  254.3 40.0 reduce-scatter.1
where the time goes:
time: 351 us; the launch traced here: 350 us
  waiting for transfers between devices  220 us (63%)
  matrix products  50.3 us (14%)
  blocking collectives  30.7 us (9%)
  starting transfers between devices  17.3 us (5%)
  between operations  14.1 us (4%)
  other arithmetic  13.2 us (4%)
  local copies, waits for them, and re-layouts  5.27 us (2%)
    all_gather x1, waiting for transfers between devices, on_device(): all_gate = lax.all_gather(gate_weight[0], 'tp', axis=0)  51.9 us
    dot_general x13, matrix products, f32dot(): return jnp.dot(a, b, preferred_element_type=jnp.float32)  49.9 us
    all_gather x1, waiting for transfers between devices, on_device(): all_up = lax.all_gather(up_weight[0], 'tp', axis=0)  39.8 us
    all_gather x1, waiting for transfers between devices, on_device(): all_down = lax.all_gather(down_weight[0], 'tp', axis=0, tiled=True)  37.1 us
    all_gather x1, waiting for transfers between devices, on_device(): lax.all_gather(arrived, 'ep', axis=0, axis_index_groups=plane_groups, til...  35.9 us
    all_to_all x1, blocking collectives, on_device(): lax.all_to_all(ordered, 'ep', split_axis=0, concat_axis=0, axis_index_gro...  30.7 us
    all_to_all x1, waiting for transfers between devices, on_device(): lax.all_to_all(home, 'ep', split_axis=0, concat_axis=0, axis_index_groups...  20.4 us
    all_to_all x1, waiting for transfers between devices, on_device(): lax.all_to_all(partial.reshape(split, -1, width), 'tp', 0, 0, tiled=True)  15.8 us
  transfers between devices with their start and end apart: 9, of which 8 were waited for; matrix products, arithmetic and copies ran while one was open for 13% of the time, Pallas kernels for 0%

commit v1 on v0

--- a/solution.py
+++ b/solution.py
@@ -5,6 +5,11 @@
 
 EPG = 8
 EPSILON = 1e-06
+
+
+def gather_by_exchange(value, axis, dim):
+    copies = jnp.concatenate([value] * lax.axis_size(axis), axis=dim)
+    return lax.all_to_all(copies, axis, dim, dim, tiled=True)
 
 
 def padded_2(cells, axis):
@@ -90,7 +95,7 @@
     everyone = lax.all_gather(arrived, "ep", axis=0, axis_index_groups=plane_groups, tiled=True)
     all_gate = lax.all_gather(gate_weight[0], "tp", axis=0)
     all_up = lax.all_gather(up_weight[0], "tp", axis=0)
-    all_down = lax.all_gather(down_weight[0], "tp", axis=0, tiled=True)
+    all_down = gather_by_exchange(down_weight[0], "tp", 0)
     normal_rows = normed(mixer_input, mixer_gain)
     values = f32dot(normal_rows, value_weight)
     inner = f32dot(normal_rows, inner_gate)

time: 351 us -> 290 us (0.83)
  waiting for transfers between devices: 220 us -> 147 us
  starting transfers between devices: 17.3 us -> 22.3 us
    all_gather x1, waiting for transfers between devices: 51.9 us -> 5.95 us  [on_device(): all_gate = lax.all_gather(gate_weight[0], 'tp', axis=0)]
    all_gather x1 -> x0, waiting for transfers between devices: 37.1 us -> none  [on_device(): all_down = lax.all_gather(down_weight[0], 'tp', axis=0, tiled=True)]
    all_gather x1, waiting for transfers between devices: 35.9 us -> 47.4 us  [on_device(): lax.all_gather(arrived, 'ep', axis=0, axis_index_groups=plane_groups, til...]
    all_to_all x0 -> x1, starting transfers between devices: none -> 4.87 us  [gather_by_exchange(): return lax.all_to_all(copies, axis, dim, dim, tiled=True)]
    concatenate x0 -> x1, other arithmetic: none -> 4.09 us  [gather_by_exchange(): copies = jnp.concatenate([value] * lax.axis_size(axis), axis=dim)]
  transfers between devices with their start and end apart: 9 -> 9, of which waited for: 8 -> 7; matrix products, arithmetic and copies ran while one was open for 13% -> 21% of each run, Pallas kernels for 0% -> 0%
where the time goes in v1:
time: 290 us; the launch traced here: 289 us
  waiting for transfers between devices  147 us (51%)
  matrix products  52.9 us (18%)
  blocking collectives  30.7 us (11%)
  starting transfers between devices  22.3 us (8%)
  other arithmetic  16.3 us (6%)
  between operations  14 us (5%)
  local copies, waits for them, and re-layouts  5.28 us (2%)
    dot_general x13, matrix products, f32dot(): return jnp.dot(a, b, preferred_element_type=jnp.float32)  52.4 us
    all_gather x1, waiting for transfers between devices, on_device(): lax.all_gather(arrived, 'ep', axis=0, axis_index_groups=plane_groups, til...  47.4 us
    all_gather x1, waiting for transfers between devices, on_device(): all_up = lax.all_gather(up_weight[0], 'tp', axis=0)  39.7 us
    all_to_all x1, blocking collectives, on_device(): lax.all_to_all(ordered, 'ep', split_axis=0, concat_axis=0, axis_index_gro...  30.7 us
    all_to_all x1, waiting for transfers between devices, on_device(): lax.all_to_all(home, 'ep', split_axis=0, concat_axis=0, axis_index_groups...  20.4 us
    all_to_all x1, waiting for transfers between devices, on_device(): lax.all_to_all(partial.reshape(split, -1, width), 'tp', 0, 0, tiled=True)  15.8 us
    reduce_scatter x1, waiting for transfers between devices, on_device(): lax.psum_scatter(answers, 'ep', scatter_dimension=0, axis_index_groups=pl...  13.4 us
    all_to_all x1, starting transfers between devices, on_device(): lax.all_to_all(home, 'ep', split_axis=0, concat_axis=0, axis_index_groups...  6.72 us
  transfers between devices with their start and end apart: 9, of which 7 were waited for; matrix products, arithmetic and copies ran while one was open for 21% of the time, Pallas kernels for 0%

profile of v1, /device:TPU:3, one launch (start us, length us, event | category | flops | bytes accessed | tf_op | source)
XLA Modules:
  0.0 289.0 jit_solution(1430096890312880267)
XLA Ops:
  7.2 0.0 copy-start
  7.2 0.0 all-gather.6.cloned.1.call-start
  7.2 0.7 all-gather.6.cloned.1.call-update
  7.9 0.0 all-gather.4.cloned.1.call-start
  8.0 0.7 rev.3
  8.7 0.7 fusion.51
  9.4 0.7 select_reduce_fusion.1
  10.1 0.7 exponential_reduce_fusion
  10.8 0.7 and_select_fusion
  11.5 0.7 divide_multiply_fusion
  12.2 0.1 copy.23
  12.4 0.1 copy.24
  12.5 1.3 fusion.14
  13.8 1.3 fusion.16
  15.2 0.3 concatenate.13
  15.5 0.2 convert_reduce_fusion
  15.7 0.5 convolution_convert_fusion
  16.1 0.1 all_to_all.28
  16.3 30.7 %all_to_all.41 = bf16[8,20,2176]{2,1,0:T(8,128)(2,1)S(1)} all-to-all(bf16[8,20,2176]{2,1,0:T(8,128)(2,1)S(1)} %all_to_all.28), channel_id=1, replica_groups={{0,32,64,96,128,160,192,224},{4,36,68,100,132,164,196,228},{8,40,72,104..., dimensions={0} | all-to-all | bytes 1392640 | tf_op jit(solution)/shard_map/all_to_all | solution.py:92
  47.0 1.0 all_to_all.30
  48.0 0.0 all-gather.4.cloned.1.call-update
  48.0 0.0 all-gather.8.cloned.1.call-start
  48.1 0.7 all-gather.8.cloned.1.call-update
  48.8 4.1 %pad_maximum_fusion = bf16[1024,2048]{1,0:T(8,128)(2,1)} fusion(bf16[256,2048]{1,0:T(8,128)(2,1)} %bitcast.48), kind=kLoop, calls=%fused_computation.6 | loop fusion | flops 16777216 | bytes 5242880 | tf_op jit(solution)/shard_map/concatenate | solution.py:11
  52.9 4.9 %all-to-all-start.2 = ((bf16[4,256,2048]{2,1,0:T(8,128)(2,1)}), bf16[4,256,2048]{2,1,0:T(8,128)(2,1)}, u32[]{:S(2)}, u32[]{:S(2)}) async-start(bf16[4,256,2048]{2,1,0:T(8,128)(2,1)} %bitcast.46), calls=%async_computation.2 | async-start | bytes 8388608 | tf_op jit(solution)/shard_map/all_to_all | solution.py:12
  57.7 0.2 reduce-scatter.2.cloned.1.call-start
  58.0 6.0 %all-gather.6.cloned.1.call-done = bf16[4,2048,256]{2,1,0:T(8,128)(2,1)} async-done(((bf16[1,2048,256]{2,1,0:T(8,128)(2,1)}), bf16[4,2048,256]{2,1,0:T(8,128)(2,1)}) %all-gather.6.cloned.1.call-update) | async-done | bytes 4194320 | tf_op jit(solution)/shard_map/all_gather | solution.py:96
  64.0 47.4 %all-gather.4.cloned.1.call-done = bf16[1280,2176]{1,0:T(8,128)(2,1)} async-done(((bf16[160,2176]{1,0:T(8,128)(2,1)}), bf16[1280,2176]{1,0:T(8,128)(2,1)}) %all-gather.4.cloned.1.call-update) | async-done | bytes 5570576 | tf_op jit(solution)/shard_map/all_gather | solution.py:95
  111.4 5.5 %fusion.22 = f32[1280,256]{0,1:T(8,128)} fusion(bf16[4,2048,256]{2,1,0:T(8,128)(2,1)} %all-gather.6.cloned.1.call-done, bf16[1280,2176]{1,0:T(8,128)(2,1)} %all-gather.4.cloned.1.call-done), kind=kOutput, calls=%fused_computation.45 | convolution fusion | flops 1342177280 | bytes 7602176 | tf_op jit(solution)/shard_map/dot_general | solution.py:45
  116.9 0.6 copy-done.4
  117.5 2.7 fusion.21
  120.2 2.7 fusion.20
  122.9 1.6 fusion.19
  124.5 0.2 select_reduce_fusion
  124.7 39.7 %all-gather.8.cloned.1.call-done = bf16[4,2048,256]{2,1,0:T(8,128)(2,1)} async-done(((bf16[1,2048,256]{2,1,0:T(8,128)(2,1)}), bf16[4,2048,256]{2,1,0:T(8,128)(2,1)}) %all-gather.8.cloned.1.call-update) | async-done | bytes 4194320 | tf_op jit(solution)/shard_map/all_gather | solution.py:97
  164.4 5.0 %fusion.10 = bf16[1280,256]{0,1:T(8,128)(2,1)S(1)} fusion(f32[1280,256]{0,1:T(8,128)} %fusion.22, bf16[4,2048,256]{2,1,0:T(8,128)(2,1)} %all-gather.8.cloned.1.call-done, bf16[1280,2176]{1,0:T(8,128)(2,1)} %all-gather.4.cloned.1.call-done), kind=kOutput, calls=%fused_computation.20 | convolution fusion | flops 1344143360 | bytes 8257536 | tf_op jit(solution)/shard_map/dot_general | solution.py:45
  169.4 0.0 slice-start
  169.4 5.2 %fusion.11 = bf16[1280,256]{0,1:T(8,128)(2,1)} fusion(f32[1280,256]{0,1:T(8,128)S(1)} %copy-done.9, bf16[4,2048,256]{2,1,0:T(8,128)(2,1)S(1)} %copy-done.5, bf16[1280,2176]{1,0:T(8,128)(2,1)} %all-gather.4.cloned.1.call-done), kind=kOutput, calls=%fused_computation.21 | convolution fusion | flops 1344143360 | bytes 8257536 | tf_op jit(solution)/shard_map/dot_general | solution.py:45
  174.7 5.2 %fusion.12 = bf16[1280,256]{0,1:T(8,128)(2,1)} fusion(f32[1280,256]{0,1:T(8,128)S(1)} %copy-done.8, bf16[4,2048,256]{2,1,0:T(8,128)(2,1)S(1)} %copy-done.5, bf16[1280,2176]{1,0:T(8,128)(2,1)} %all-gather.4.cloned.1.call-done), kind=kOutput, calls=%fused_computation.22 | convolution fusion | flops 1344143360 | bytes 8257536 | tf_op jit(solution)/shard_map/dot_general | solution.py:45
  179.9 2.9 fusion.13
  182.7 0.0 all-to-all-done.2
  182.7 9.9 %multiply_convert_fusion = bf16[1280,2048]{1,0:T(8,128)(2,1)} fusion(bf16[1024,2048]{1,0:T(8,128)(2,1)} %bitcast.22, f32[1280]{0:T(1024)S(1)} %select_reduce_fusion, bf16[1280,256]{0,1:T(8,128)(2,1)} %fusion.13, bf16[1280,256]{0,1:T(8,128)(2,1)} %fusion.12, bf16[1280,256]{0,1:T(8,128)(2,1)} %fusion.11, bf16[1280,256]{0,1:T(8,128)(2,1)S(1)} %fusion.10), kind=kOutput, calls=%fused_computation | convolution fusion | flops 5384437760 | bytes 12063744 | tf_op jit(solution)/shard_map/dot_general | solution.py:45
  192.7 0.0 reduce-scatter.2.cloned.1.call-update
  192.7 2.3 fusion
  195.0 0.0 copy-start.1
  195.0 0.0 copy-start.6
  195.0 3.1 %fusion.45 = f32[640,256]{1,0:T(8,128)S(1)} fusion(bf16[2048,256]{1,0:T(8,128)(2,1)} %param.18, bf16[640,2048]{1,0:T(8,128)(2,1)} %param.15, f32[2048]{0:T(1024)S(1)} %copy-done.7, f32[640]{0:T(1024)S(1)} %add_rsqrt_fusion), kind=kOutput, calls=%fused_computation.97 | convolution fusion | flops 676331520 | bytes 4336128 | tf_op jit(solution)/shard_map/dot_general | solution.py:45
  198.1 0.0 copy-done.6
  198.1 0.9 fusion.18
  199.1 3.8 %collective-permute-start = (bf16[1,256]{1,0:T(2,128)(2,1)S(1)}, bf16[1,256]{1,0:T(2,128)(2,1)S(1)}, u32[]{:S(2)}, u32[]{:S(2)}) collective-permute-start(bf16[1,256]{1,0:T(2,128)(2,1)S(1)} %get-tuple-element.2), channel_id=1, source_target_pairs={{0,4},{4,8},{8,12},{12,16},{16,20},{20,24},{24,28},{28,32},{32,36}... | collective-permute-start | bytes 1544 | tf_op jit(solution)/shard_map/ppermute | solution.py:22
  202.9 1.9 collective-permute-start.1
  204.9 0.0 collective-permute-done
  204.9 3.3 %collective-permute-done.1 = bf16[1,256]{1,0:T(2,128)(2,1)S(1)} collective-permute-done((bf16[1,256]{1,0:T(2,128)(2,1)S(1)}, bf16[1,256]{1,0:T(2,128)(2,1)S(1)}, u32[]{:S(2)}, u32[]{:S(2)}) %collective-permute-start.1) | collective-permute-done | bytes 544 | tf_op jit(solution)/shard_map/ppermute | solution.py:24
  208.2 0.1 maximum_convert_fusion
  208.3 6.5 %convolution_convert_fusion.1 = bf16[640,2048]{1,0:T(8,128)(2,1)} fusion(bf16[256,2048]{1,0:T(8,128)(2,1)S(1)} %copy-done, bf16[2048,256]{1,0:T(8,128)(2,1)} %param.19, f32[642,256]{1,0:T(8,128)S(1)} %maximum_convert_fusion, f32[256]{0:T(256)S(1)} %bitcast.62, f32[256]{0:T(256)S(1)} %bitcast.63, f32[256]{0:T(256)S(1)} %bitcast.61, ...), kind=kOutput, calls=%fused_computation.8 | convolution fusion | flops 1349877760 | bytes 9321472 | tf_op jit(solution)/shard_map/dot_general | solution.py:45
  214.8 4.6 %all-to-all-start = ((bf16[4,160,2048]{2,1,0:T(8,128)(2,1)}), bf16[4,160,2048]{2,1,0:T(8,128)(2,1)}, u32[]{:S(2)}, u32[]{:S(2)}) async-start(bf16[4,160,2048]{2,1,0:T(8,128)(2,1)} %bitcast.47), calls=%async_computation | async-start | bytes 5242880 | tf_op jit(solution)/shard_map/all_to_all | solution.py:110
  219.4 13.4 %reduce-scatter.2.cloned.1.call-done = bf16[160,2048]{1,0:T(8,128)(2,1)} async-done(((bf16[1280,2048]{1,0:T(8,128)(2,1)}), bf16[160,2048]{1,0:T(8,128)(2,1)}) %reduce-scatter.2.cloned.1.call-update) | async-done | bytes 655376 | tf_op jit(solution)/shard_map/reduce_scatter | solution.py:126
  232.9 2.0 all_to_all.34
  234.9 15.8 %all-to-all-done = bf16[4,160,2048]{2,1,0:T(8,128)(2,1)} async-done(((bf16[4,160,2048]{2,1,0:T(8,128)(2,1)}), bf16[4,160,2048]{2,1,0:T(8,128)(2,1)}, u32[]{:S(2)}, u32[]{:S(2)}) %all-to-all-start) | async-done | bytes 2621472 | tf_op jit(solution)/shard_map/all_to_all | solution.py:110
  250.7 6.7 %all-to-all-start.3 = ((bf16[8,20,2048]{2,1,0:T(8,128)(2,1)}), bf16[8,20,2048]{2,1,0:T(8,128)(2,1)S(1)}, u32[]{:S(2)}, u32[]{:S(2)}) async-start(bf16[8,20,2048]{2,1,0:T(8,128)(2,1)} %all_to_all.34), calls=%async_computation.4 | async-start | bytes 1572864 | tf_op jit(solution)/shard_map/all_to_all | solution.py:129
  257.4 3.3 %reduce_sum.69 = bf16[160,2048]{1,0:T(8,128)(2,1)} reduce(bf16[4,160,2048]{2,1,0:T(8,128)(2,1)} %all-to-all-done, bf16[]{:T(256)} %constant.55.clone.1), dimensions={0}, to_apply=%region_1.2 | reduce | flops 983040 | bytes 3276802 | tf_op jit(solution)/shard_map/reduce_sum | solution.py:111
  260.7 20.4 %all-to-all-done.3 = bf16[8,20,2048]{2,1,0:T(8,128)(2,1)S(1)} async-done(((bf16[8,20,2048]{2,1,0:T(8,128)(2,1)}), bf16[8,20,2048]{2,1,0:T(8,128)(2,1)S(1)}, u32[]{:S(2)}, u32[]{:S(2)}) %all-to-all-start.3) | async-done | bytes 655392 | tf_op jit(solution)/shard_map/all_to_all | solution.py:129
  281.1 0.1 all_to_all.36
  281.2 1.2 convolution_convert_fusion.2
  (31 shorter events, 0.1 us)
Async XLA Ops:
  7.2 201.1 %copy-start = (bf16[256,2048]{1,0:T(8,128)(2,1)S(1)}, bf16[256,2048]{1,0:T(8,128)(2,1)}, u32[]{:S(2)}) copy-start(bf16[256,2048]{1,0:T(8,128)(2,1)} %param.21) | copy-start | bytes 3145732
  7.2 56.8 %all-gather.6.cloned.1.call-start = ((), (), s32[]{:S(2)}) async-start(), calls=%async_computation.6 | async-start | bytes 5242880 | tf_op jit(solution)/shard_map/all_gather | solution.py:96
  7.9 103.4 %all-gather.4.cloned.1.call-start = ((), (), s32[]{:S(2)}) async-start(), calls=%async_computation.5 | async-start | bytes 6266880 | tf_op jit(solution)/shard_map/all_gather | solution.py:95
  48.0 116.4 %all-gather.8.cloned.1.call-start = ((), (), s32[]{:S(2)}) async-start(), calls=%async_computation.7 | async-start | bytes 5242880 | tf_op jit(solution)/shard_map/all_gather | solution.py:97
  52.9 129.9 %all-to-all-start.2 = ((bf16[4,256,2048]{2,1,0:T(8,128)(2,1)}), bf16[4,256,2048]{2,1,0:T(8,128)(2,1)}, u32[]{:S(2)}, u32[]{:S(2)}) async-start(bf16[4,256,2048]{2,1,0:T(8,128)(2,1)} %bitcast.46), calls=%async_computation.2 | async-start | bytes 8388608 | tf_op jit(solution)/shard_map/all_to_all | solution.py:12
  57.7 175.1 %reduce-scatter.2.cloned.1.call-start = ((), (), s32[]{:S(2)}) async-start(), calls=%async_computation.8 | async-start | bytes 5898240 | tf_op jit(solution)/shard_map/reduce_scatter | solution.py:126
  111.4 5.6 %copy-start.2 = (bf16[1280,2176]{1,0:T(8,128)(2,1)S(1)}, bf16[1280,2176]{1,0:T(8,128)(2,1)}, u32[]{:S(2)}) copy-start(bf16[1280,2176]{1,0:T(8,128)(2,1)} %all-gather.4.cloned.1.call-done) | copy-start | bytes 16711684
  111.4 6.1 %copy-start.4 = (bf16[4,2048,256]{2,1,0:T(8,128)(2,1)S(1)}, bf16[4,2048,256]{2,1,0:T(8,128)(2,1)}, u32[]{:S(2)}) copy-start(bf16[4,2048,256]{2,1,0:T(8,128)(2,1)} %all-gather.6.cloned.1.call-done) | copy-start | bytes 12582916
  164.4 5.0 %copy-start.5 = (bf16[4,2048,256]{2,1,0:T(8,128)(2,1)S(1)}, bf16[4,2048,256]{2,1,0:T(8,128)(2,1)}, u32[]{:S(2)}) copy-start(bf16[4,2048,256]{2,1,0:T(8,128)(2,1)} %all-gather.8.cloned.1.call-done) | copy-start | bytes 12582916
  164.4 5.0 %copy-start.9 = (f32[1280,256]{0,1:T(8,128)S(1)}, f32[1280,256]{0,1:T(8,128)}, u32[]{:S(2)}) copy-start(f32[1280,256]{0,1:T(8,128)} %fusion.21) | copy-start | bytes 3932164
  169.4 5.2 %copy-start.8 = (f32[1280,256]{0,1:T(8,128)S(1)}, f32[1280,256]{0,1:T(8,128)}, u32[]{:S(2)}) copy-start(f32[1280,256]{0,1:T(8,128)} %fusion.20) | copy-start | bytes 3932164
  169.4 10.4 %slice-start = ((s8[5570560]{0:T(1024)(128)(4,1)}), s8[4194304]{0:T(1024)(128)(4,1)S(1)}, s32[]{:S(2)}) async-start(s8[5570560]{0:T(1024)(128)(4,1)} %bitcast.49), calls=%async_computation.9 | async-start | bytes 8388608
  174.7 5.2 %slice-start.1 = ((s8[5570560]{0:T(1024)(128)(4,1)}), s8[1376256]{0:T(1024)(128)(4,1)S(1)}, s32[]{:S(2)}) async-start(s8[5570560]{0:T(1024)(128)(4,1)} %bitcast.49), calls=%async_computation.10 | async-start | bytes 2752512
  192.7 2.4 copy-start.7
  195.0 3.1 %copy-start.1 = (bf16[640,2048]{1,0:T(8,128)(2,1)S(1)}, bf16[640,2048]{1,0:T(8,128)(2,1)}, u32[]{:S(2)}) copy-start(bf16[640,2048]{1,0:T(8,128)(2,1)} %param.15) | copy-start | bytes 7864324
  195.0 3.1 %copy-start.6 = (bf16[2048,256]{1,0:T(8,128)(2,1)S(1)}, bf16[2048,256]{1,0:T(8,128)(2,1)}, u32[]{:S(2)}) copy-start(bf16[2048,256]{1,0:T(8,128)(2,1)} %param.17) | copy-start | bytes 3145732
  198.1 6.7 %copy-start.3 = (f32[3,256]{1,0:T(4,128)S(1)}, f32[3,256]{1,0:T(4,128)}, u32[]{:S(2)}) copy-start(f32[3,256]{1,0:T(4,128)} %param.20) | copy-start | bytes 9220
  199.1 5.8 %collective-permute-start = (bf16[1,256]{1,0:T(2,128)(2,1)S(1)}, bf16[1,256]{1,0:T(2,128)(2,1)S(1)}, u32[]{:S(2)}, u32[]{:S(2)}) collective-permute-start(bf16[1,256]{1,0:T(2,128)(2,1)S(1)} %get-tuple-element.2), channel_id=1, source_target_pairs={{0,4},{4,8},{8,12},{12,16},{16,20},{20,24},{24,28},{28,32},{32,36}... | collective-permute-start | bytes 1544 | tf_op jit(solution)/shard_map/ppermute | solution.py:22
  202.9 5.3 %collective-permute-start.1 = (bf16[1,256]{1,0:T(2,128)(2,1)S(1)}, bf16[1,256]{1,0:T(2,128)(2,1)S(1)}, u32[]{:S(2)}, u32[]{:S(2)}) collective-permute-start(bf16[1,256]{1,0:T(2,128)(2,1)S(1)} %get-tuple-element.3), channel_id=1, source_target_pairs={{4,0},{8,4},{12,8},{16,12},{20,16},{24,20},{28,24},{32,28},{36,32}... | collective-permute-start | bytes 1544 | tf_op jit(solution)/shard_map/ppermute | solution.py:24
  214.8 35.9 %all-to-all-start = ((bf16[4,160,2048]{2,1,0:T(8,128)(2,1)}), bf16[4,160,2048]{2,1,0:T(8,128)(2,1)}, u32[]{:S(2)}, u32[]{:S(2)}) async-start(bf16[4,160,2048]{2,1,0:T(8,128)(2,1)} %bitcast.47), calls=%async_computation | async-start | bytes 5242880 | tf_op jit(solution)/shard_map/all_to_all | solution.py:110
  250.7 30.4 %all-to-all-start.3 = ((bf16[8,20,2048]{2,1,0:T(8,128)(2,1)}), bf16[8,20,2048]{2,1,0:T(8,128)(2,1)S(1)}, u32[]{:S(2)}, u32[]{:S(2)}) async-start(bf16[8,20,2048]{2,1,0:T(8,128)(2,1)} %all_to_all.34), calls=%async_computation.4 | async-start | bytes 1572864 | tf_op jit(solution)/shard_map/all_to_all | solution.py:129
Sparse Core Ops, SparseCore 0:
  9.8 54.1 all-gather.5
  65.8 45.5 all-gather.3
  113.2 51.1 all-gather.7
  192.8 40.0 reduce-scatter.1
